TPU v7x, 256 devices: a whole 4x4x8 slice. The times are simulated.
256 devices in a mesh: sp: 32 (over z, y), dp: 8 (over x, core).
Axes of the slice: x: 4, y: 4, z: 8, core: 2. Of those that a mesh axis runs over, the one named last changes fastest.
Arguments:
- queries: bfloat16 [32768, 6144], P(('dp', 'sp')), may hold values from -360 to 360
- latent: bfloat16 [32768, 1024], P(('dp', 'sp')), may hold values from -6 to 6
- rope_key: bfloat16 [32768, 64], P(('dp', 'sp')), may hold values from -6 to 6
- latent_gain: float32 [1024], replicated, may hold values from 0.1 to 1.9
- kv_weight: bfloat16 [1024, 8192], P(None, 'dp'), may hold values from -0.1875 to 0.1875
- gate: bfloat16 [32768, 4096], P(('dp', 'sp')), may hold values from -6 to 6
- out_gain: float32 [4096], replicated, may hold values from 0.1 to 1.9
Outputs:
- attended: bfloat16 [32768, 4096], P(('dp', 'sp'))
All inputs are finite; a program needn't handle non-finite values.
Results may differ from a plain program's by a relative error of at most 0.007.
Values may be sent and summed in bfloat16 or wider, within the bound.
A program may use at most 128 MiB of HBM per device.

v0:
```python
import jax
import jax.numpy as jnp
from jax import lax
from jax.sharding import PartitionSpec as P

HEADS = 32
NOPE = 128
ROPE = 64
VDIM = 128
EPS = 1e-06
THETA = 10000.0


def in_order(blocks, dim):
    blocks = jnp.moveaxis(blocks, 0, dim)
    shape = blocks.shape
    return blocks.reshape(*shape[:dim], shape[dim] * shape[dim + 1], *shape[dim + 2 :])


def copy_for_each(value, axis):
    length = lax.axis_size(axis)
    return lax.all_to_all(
        jnp.broadcast_to(value[None], (length, *value.shape)), axis, 0, 0, tiled=True
    )


def gathered_copies(value, axis, dim):
    return in_order(copy_for_each(value, axis), dim)


def rotary(values, position):
    half_width = values.shape[-1] // 2
    inverse = THETA ** (-jnp.arange(half_width, dtype=jnp.float32) / half_width)
    angles = position.astype(jnp.float32)[:, None] * inverse[None, :]
    if values.ndim == 3:
        angles = angles[:, None, :]
    cosine = jnp.cos(angles)
    sine_part = jnp.sin(angles)
    front_half = values[..., :half_width].astype(jnp.float32)
    back_half = values[..., half_width:].astype(jnp.float32)
    turned = jnp.concatenate(
        [front_half * cosine - back_half * sine_part, back_half * cosine + front_half * sine_part],
        axis=-1,
    )
    return turned.astype(jnp.bfloat16)


def attend(query_block, keys_plain, keys_rotated, values):
    scores = jnp.einsum(
        "qhd,khd->hqk", query_block[..., :NOPE], keys_plain, preferred_element_type=jnp.float32
    )
    scores = scores + jnp.einsum(
        "qhr,kr->hqk", query_block[..., NOPE:], keys_rotated, preferred_element_type=jnp.float32
    )
    scores = scores * (NOPE + ROPE) ** (-0.5)
    row_max = jnp.max(scores, axis=-1, keepdims=True)
    raised = jnp.exp(scores - row_max)
    weights = (raised / jnp.sum(raised, axis=-1, keepdims=True)).astype(jnp.bfloat16)
    result = jnp.einsum("hqk,khd->qhd", weights, values, preferred_element_type=jnp.float32)
    return result.astype(jnp.bfloat16)


def per_device(queries, latent, rope_key, latent_gain, kv_weight, gate, out_gain):
    own_tokens = queries.shape[0]
    groups = lax.axis_size("sp")
    seq_len = own_tokens * groups
    offset = lax.axis_index("sp") * own_tokens
    position = offset + jnp.arange(own_tokens, dtype=jnp.int32)
    widened = latent.astype(jnp.float32)
    normed = (
        widened * lax.rsqrt(jnp.mean(widened * widened, axis=-1, keepdims=True) + EPS) * latent_gain
    ).astype(jnp.bfloat16)
    keyval = jnp.dot(
        normed,
        lax.all_gather(kv_weight, "dp", axis=1, tiled=True),
        preferred_element_type=jnp.float32,
    ).astype(jnp.bfloat16)
    head_queries = queries.reshape(own_tokens, HEADS, NOPE + ROPE)
    head_queries = jnp.concatenate(
        [head_queries[..., :NOPE], rotary(head_queries[..., NOPE:], position)], axis=-1
    )
    head_queries = head_queries.reshape(own_tokens, HEADS * (NOPE + ROPE))
    rotated_all = gathered_copies(rotary(rope_key, position), "sp", 0)
    query_all, kv_all = (
        lax.all_to_all(head_queries, "sp", split_axis=1, concat_axis=0, tiled=True),
        lax.all_to_all(keyval, "sp", split_axis=1, concat_axis=0, tiled=True),
    )
    local_heads = HEADS // groups
    rows_all = query_all.shape[0]
    seq_count = rows_all // seq_len
    block_rows = min(512, seq_len)
    block_count = seq_len // block_rows

    def one_sequence(operands):
        query_seq, kv_seq, rope_seq = operands
        keys_plain = kv_seq[..., :NOPE]
        values = kv_seq[..., NOPE:]
        blocks = query_seq.reshape(block_count, block_rows, local_heads, NOPE + ROPE)
        result = lax.map(
            lambda piece_rows: attend(piece_rows, keys_plain, rope_seq, values), blocks
        )
        return result.reshape(seq_len, local_heads * VDIM)

    heads_out = lax.map(
        one_sequence,
        (
            query_all.reshape(seq_count, seq_len, local_heads, NOPE + ROPE),
            kv_all.reshape(seq_count, seq_len, local_heads, NOPE + VDIM),
            rotated_all.reshape(seq_count, seq_len, ROPE),
        ),
    )
    heads_out = heads_out.reshape(rows_all, local_heads * VDIM)
    token_rows = lax.all_to_all(heads_out, "sp", split_axis=0, concat_axis=1, tiled=True)
    gated_rows = token_rows.astype(jnp.float32) * jax.nn.silu(gate.astype(jnp.float32))
    scale_rows = lax.rsqrt(jnp.mean(gated_rows * gated_rows, axis=-1, keepdims=True) + EPS)
    return (gated_rows * scale_rows * out_gain).astype(jnp.bfloat16)


def solution(mesh):
    return jax.shard_map(
        per_device,
        mesh=mesh,
        in_specs=(
            P(("dp", "sp"), None),
            P(("dp", "sp"), None),
            P(("dp", "sp"), None),
            P(),
            P(None, "dp"),
            P(("dp", "sp"), None),
            P(),
        ),
        out_specs=P(("dp", "sp"), None),
        check_vma=False,
    )
```

profile of v0, /device:TPU:8, one launch (start us, length us, event | category | flops | bytes accessed | tf_op | source)
XLA Modules:
  0.0 278.0 jit_solution(5976931859334378445)
XLA Ops:
  7.5 0.9 broadcast_in_dim.7
  8.4 11.7 %all-to-all-start.2 = ((bf16[32,128,64]{1,2,0:T(8,128)(2,1)}), bf16[32,128,64]{1,2,0:T(8,128)(2,1)S(1)}, u32[]{:S(2)}, u32[]{:S(2)}) async-start(bf16[32,128,64]{1,2,0:T(8,128)(2,1)} %broadcast_in_dim.7), calls=%async_computation.2 | async-start | bytes 1048576 | tf_op jit(solution)/shard_map/all_to_all | solution.py:22
  20.1 1.9 copy.26
  22.3 1.3 pad_maximum_fusion
  23.6 13.3 %all-to-all-done.2 = bf16[32,128,64]{1,2,0:T(8,128)(2,1)S(1)} async-done(((bf16[32,128,64]{1,2,0:T(8,128)(2,1)}), bf16[32,128,64]{1,2,0:T(8,128)(2,1)S(1)}, u32[]{:S(2)}, u32[]{:S(2)}) %all-to-all-start.2) | async-done | bytes 524320 | tf_op jit(solution)/shard_map/all_to_all | solution.py:22
  36.9 5.6 %all-to-all-start = ((bf16[128,32,192]{0,2,1:T(8,128)(2,1)}), bf16[128,32,192]{0,2,1:T(8,128)(2,1)S(1)}, u32[]{:S(2)}, u32[]{:S(2)}) async-start(bf16[128,32,192]{0,2,1:T(8,128)(2,1)} %pad_maximum_fusion), calls=%async_computation | async-start | bytes 3145728 | tf_op jit(solution)/shard_map/all_to_all | solution.py:85
  42.6 56.9 %all-gather.2.cloned.1.call-done = bf16[1024,8192]{1,0:T(8,128)(2,1)} async-done(((bf16[1024,1024]{1,0:T(8,128)(2,1)}), bf16[1024,8192]{1,0:T(8,128)(2,1)}) %all-gather.2.cloned.1.call-update) | async-done | bytes 16777232 | tf_op jit(solution)/shard_map/all_gather | solution.py:75
  99.5 8.2 %convolution_convert_fusion = bf16[128,8192]{1,0:T(8,128)(2,1)S(1)} fusion(bf16[1024,8192]{1,0:T(8,128)(2,1)} %all-gather.2.cloned.1.call-done, bf16[128,1024]{1,0:T(8,128)(2,1)S(1)} %copy-done.3, f32[1024]{0:T(1024)S(1)} %copy-done.8, f32[128]{0:T(128)S(1)} %add_rsqrt_fusion.1), kind=kOutput, calls=%fused_computation.16 | convolution fusion | flops 2149056512 | bytes 19141120 | tf_op jit(solution)/shard_map/dot_general | solution.py:73
  107.7 1.6 copy.39
  109.3 1.2 copy-done.1
  110.5 10.2 %all-to-all-start.1 = ((bf16[128,32,256]{2,0,1:T(8,128)(2,1)}), bf16[128,32,256]{2,0,1:T(8,128)(2,1)S(1)}, u32[]{:S(2)}, u32[]{:S(2)}) async-start(bf16[128,32,256]{2,0,1:T(8,128)(2,1)} %bitcast.86), calls=%async_computation.1 | async-start | bytes 4194304 | tf_op jit(solution)/shard_map/all_to_all | solution.py:86
  120.6 1.5 copy.35
  122.2 3.6 %copy.27 = bf16[32,128,192]{1,0,2:T(8,128)(2,1)} copy(bf16[32,128,192]{1,2,0:T(8,128)(2,1)} %bitcast.88) | data formatting | bytes 3145728 | tf_op jit(solution)/shard_map/all_to_all | solution.py:85
  125.7 3.7 %reshape.157 = bf16[8,512,1,192]{1,0,3,2:T(8,128)(2,1)} reshape(bf16[32,128,192]{1,0,2:T(8,128)(2,1)} %copy.27) | data formatting | bytes 3145728 | tf_op jit(solution)/shard_map/while/body/eval_jaxpr/reshape | solution.py:98
  129.5 3.1 %copy.30 = bf16[8,512,1,192]{1,3,2,0:T(8,128)(2,1)} copy(bf16[8,512,1,192]{1,0,3,2:T(8,128)(2,1)} %reshape.157) | data formatting | bytes 3145728 | tf_op jit(solution)/shard_map/while/body/eval_jaxpr/while | solution.py:99
  132.5 37.7 %all-to-all-done.1 = bf16[128,32,256]{2,0,1:T(8,128)(2,1)S(1)} async-done(((bf16[128,32,256]{2,0,1:T(8,128)(2,1)}), bf16[128,32,256]{2,0,1:T(8,128)(2,1)S(1)}, u32[]{:S(2)}, u32[]{:S(2)}) %all-to-all-start.1) | async-done | bytes 2097184 | tf_op jit(solution)/shard_map/all_to_all | solution.py:86
  170.2 1.3 copy-done
  171.6 2.7 fusion.35
  174.3 57.8 %while.17 = (s32[]{:T(128)}, bf16[8,512,1,128]{3,1,2,0:T(8,128)(2,1)S(1)}, bf16[8,512,1,192]{1,3,2,0:T(8,128)(2,1)}, bf16[4096,1,128]{2,0,1:T(8,128)(2,1)S(1)}, ...) while((s32[]{:T(128)}, bf16[8,512,1,128]{3,1,2,0:T(8,128)(2,1)S(1)}, ...), condition=%wide.region_4.5_spmd, body=%wide.region_1.4_spmd.sunk | while | flops 1359019008 | bytes 50014328 | solution.py:99
  174.3 0.9 dynamic-slice_bitcast_fusion.2
  175.3 1.3 fusion.50
  176.5 1.4 fusion.51
  178.0 1.3 fusion.52
  179.3 2.2 fusion.53
  181.5 0.9 dynamic-slice_bitcast_fusion.2
  182.5 1.3 fusion.50
  183.8 1.4 fusion.51
  185.2 1.3 fusion.52
  186.5 2.2 fusion.53
  188.8 0.9 dynamic-slice_bitcast_fusion.2
  189.7 1.3 fusion.50
  191.0 1.4 fusion.51
  192.4 1.3 fusion.52
  193.7 2.2 fusion.53
  196.0 0.9 dynamic-slice_bitcast_fusion.2
  196.9 1.3 fusion.50
  198.2 1.4 fusion.51
  199.7 1.3 fusion.52
  200.9 2.2 fusion.53
  203.2 0.9 dynamic-slice_bitcast_fusion.2
  204.2 1.3 fusion.50
  205.4 1.4 fusion.51
  206.9 1.3 fusion.52
  208.2 2.2 fusion.53
  210.4 0.9 dynamic-slice_bitcast_fusion.2
  211.4 1.3 fusion.50
  212.7 1.4 fusion.51
  214.1 1.3 fusion.52
  215.4 2.2 fusion.53
  217.7 0.9 dynamic-slice_bitcast_fusion.2
  218.6 1.3 fusion.50
  219.9 1.4 fusion.51
  221.3 1.3 fusion.52
  222.6 2.2 fusion.53
  224.9 0.9 dynamic-slice_bitcast_fusion.2
  225.8 1.3 fusion.50
  227.1 1.4 fusion.51
  228.6 1.3 fusion.52
  229.8 2.2 fusion.53
  232.1 0.9 copy-done.6
  233.1 6.3 %all-to-all-start.3 = ((bf16[32,128,128]{2,1,0:T(8,128)(2,1)}), bf16[32,128,128]{2,1,0:T(8,128)(2,1)S(1)}, u32[]{:S(2)}, u32[]{:S(2)}) async-start(bf16[32,128,128]{2,1,0:T(8,128)(2,1)} %bitcast.91), calls=%async_computation.3 | async-start | bytes 2097152 | tf_op jit(solution)/shard_map/all_to_all | solution.py:113
  240.1 27.4 %all-to-all-done.3 = bf16[32,128,128]{2,1,0:T(8,128)(2,1)S(1)} async-done(((bf16[32,128,128]{2,1,0:T(8,128)(2,1)}), bf16[32,128,128]{2,1,0:T(8,128)(2,1)S(1)}, u32[]{:S(2)}, u32[]{:S(2)}) %all-to-all-start.3) | async-done | bytes 1048608 | tf_op jit(solution)/shard_map/all_to_all | solution.py:113
  268.9 0.9 multiply_convert_fusion
  269.8 1.3 copy.34
  (49 shorter events, 3.4 us)
Async XLA Ops:
  6.5 0.8 copy-start.10
  6.5 93.0 %all-gather.2.cloned.1.call-start = ((), (), s32[]{:S(2)}) async-start(), calls=%async_computation.4 | async-start | bytes 18874368 | tf_op jit(solution)/shard_map/all_gather | solution.py:75
  8.4 28.5 %all-to-all-start.2 = ((bf16[32,128,64]{1,2,0:T(8,128)(2,1)}), bf16[32,128,64]{1,2,0:T(8,128)(2,1)S(1)}, u32[]{:S(2)}, u32[]{:S(2)}) async-start(bf16[32,128,64]{1,2,0:T(8,128)(2,1)} %broadcast_in_dim.7), calls=%async_computation.2 | async-start | bytes 1048576 | tf_op jit(solution)/shard_map/all_to_all | solution.py:22
  23.6 18.9 %copy-start.3 = (bf16[128,1024]{1,0:T(8,128)(2,1)S(1)}, bf16[128,1024]{1,0:T(8,128)(2,1)}, u32[]{:S(2)}) copy-start(bf16[128,1024]{1,0:T(8,128)(2,1)} %param.10) | copy-start | bytes 786436
  23.6 75.9 %copy-start.8 = (f32[1024]{0:T(1024)S(1)}, f32[1024]{0:T(1024)}, u32[]{:S(2)}) copy-start(f32[1024]{0:T(1024)} %param.12) | copy-start | bytes 12292
  36.9 70.8 %copy-start.2 = (bf16[32,128,64]{1,2,0:T(8,128)(2,1)}, bf16[32,128,64]{1,2,0:T(8,128)(2,1)S(1)}, u32[]{:S(2)}) copy-start(bf16[32,128,64]{1,2,0:T(8,128)(2,1)S(1)} %all-to-all-done.2) | copy-start | bytes 1572868
  36.9 72.4 %all-to-all-start = ((bf16[128,32,192]{0,2,1:T(8,128)(2,1)}), bf16[128,32,192]{0,2,1:T(8,128)(2,1)S(1)}, u32[]{:S(2)}, u32[]{:S(2)}) async-start(bf16[128,32,192]{0,2,1:T(8,128)(2,1)} %pad_maximum_fusion), calls=%async_computation | async-start | bytes 3145728 | tf_op jit(solution)/shard_map/all_to_all | solution.py:85
  109.3 1.2 copy-start.1
  110.5 59.8 %all-to-all-start.1 = ((bf16[128,32,256]{2,0,1:T(8,128)(2,1)}), bf16[128,32,256]{2,0,1:T(8,128)(2,1)S(1)}, u32[]{:S(2)}, u32[]{:S(2)}) async-start(bf16[128,32,256]{2,0,1:T(8,128)(2,1)} %bitcast.86), calls=%async_computation.1 | async-start | bytes 4194304 | tf_op jit(solution)/shard_map/all_to_all | solution.py:86
  170.2 1.3 copy-start
  171.6 2.7 copy-start.5
  178.0 1.3 copy-start.7
  185.2 1.3 copy-start.7
  192.4 1.3 copy-start.7
  199.7 1.3 copy-start.7
  206.9 1.3 copy-start.7
  214.1 1.3 copy-start.7
  221.3 1.3 copy-start.7
  228.6 1.3 copy-start.7
  232.1 1.0 copy-start.6
  232.1 7.3 %copy-start.4 = (bf16[128,4096]{1,0:T(8,128)(2,1)S(1)}, bf16[128,4096]{1,0:T(8,128)(2,1)}, u32[]{:S(2)}) copy-start(bf16[128,4096]{1,0:T(8,128)(2,1)} %param.14) | copy-start | bytes 3145732
  233.1 34.4 %all-to-all-start.3 = ((bf16[32,128,128]{2,1,0:T(8,128)(2,1)}), bf16[32,128,128]{2,1,0:T(8,128)(2,1)S(1)}, u32[]{:S(2)}, u32[]{:S(2)}) async-start(bf16[32,128,128]{2,1,0:T(8,128)(2,1)} %bitcast.91), calls=%async_computation.3 | async-start | bytes 2097152 | tf_op jit(solution)/shard_map/all_to_all | solution.py:113
  240.1 28.8 %copy-start.9 = (f32[4096]{0:T(1024)S(1)}, f32[4096]{0:T(1024)}, u32[]{:S(2)}) copy-start(f32[4096]{0:T(1024)} %param.15) | copy-start | bytes 49156
Sparse Core Ops, SparseCore 0:
  9.2 90.2 all-gather.1
where the time goes:
time: 279 us; the launch traced here: 278 us
  waiting for transfers between devices  136 us (49%)
  matrix products  47.9 us (17%)
  starting transfers between devices  33.8 us (12%)
  local copies, waits for them, and re-layouts  32.8 us (12%)
  other arithmetic  13.6 us (5%)
  between operations  13.6 us (5%)
    all_gather x1, waiting for transfers between devices, per_device(): lax.all_gather(kv_weight, 'dp', axis=1, tiled=True)  56.9 us
    all_to_all x1, waiting for transfers between devices, per_device(): lax.all_to_all(keyval, 'sp', split_axis=1, concat_axis=0, tiled=True)  37.7 us
    all_to_all x1, waiting for transfers between devices, per_device(): lax.all_to_all(heads_out, 'sp', split_axis=0, concat_axis=1, tiled=True)  27.4 us
    dot_general x8, matrix products, attend(): jnp.einsum('hqk,khd->qhd', weights, values, preferred_element_type=jnp.fl...  18 us
    all_to_all x1, waiting for transfers between devices, copy_for_each(): lax.all_to_all(jnp.broadcast_to(value[None], (length, *value.shape)), axi...  13.3 us
    all_to_all x1, starting transfers between devices, copy_for_each(): lax.all_to_all(jnp.broadcast_to(value[None], (length, *value.shape)), axi...  11.7 us
    dot_general x8, matrix products, attend(): jnp.einsum('qhr,kr->hqk', query_block[..., NOPE:], keys_rotated, preferre...  11.4 us
    dot_general x8, matrix products, attend(): jnp.einsum('qhd,khd->hqk', query_block[..., :NOPE], keys_plain, preferred...  10.3 us
  transfers between devices with their start and end apart: 5, of which 4 were waited for; matrix products, arithmetic and copies ran while one was open for 10% of the time, Pallas kernels for 0%

commit v1 on v0

--- a/solution.py
+++ b/solution.py
@@ -72,7 +72,9 @@
     ).astype(jnp.bfloat16)
     keyval = jnp.dot(
         normed,
-        lax.all_gather(kv_weight, "dp", axis=1, tiled=True),
+        jnp.concatenate(
+            lax.all_to_all(jnp.stack([kv_weight] * lax.axis_size("dp")), "dp", 0, 0), axis=1
+        ),
         preferred_element_type=jnp.float32,
     ).astype(jnp.bfloat16)
     head_queries = queries.reshape(own_tokens, HEADS, NOPE + ROPE)

time: 279 us -> 426 us (1.53)
  waiting for transfers between devices: 136 us -> 282 us
  between operations: 13.6 us -> 0.21 us
  local copies, waits for them, and re-layouts: 32.8 us -> 40.5 us
    all_to_all x0 -> x1, waiting for transfers between devices: none -> 181 us  [per_device(): lax.all_to_all(jnp.stack([kv_weight] * lax.axis_size('dp')), 'dp', 0, 0)]
    all_gather x1 -> x0, waiting for transfers between devices: 56.9 us -> none  [per_device(): lax.all_gather(kv_weight, 'dp', axis=1, tiled=True)]
    all_to_all x1, waiting for transfers between devices: 0.01 us -> 25.2 us  [per_device(): lax.all_to_all(head_queries, 'sp', split_axis=1, concat_axis=0, tiled=True)]
    another operation x0 -> x1, local copies, waits for them, and re-layouts: none -> 5.96 us  [per_device(): jnp.stack([kv_weight] * lax.axis_size('dp'))]
    all_to_all x0 -> x1, starting transfers between devices: none -> 5.74 us  [per_device(): lax.all_to_all(jnp.stack([kv_weight] * lax.axis_size('dp')), 'dp', 0, 0)]
  transfers between devices with their start and end apart: 5 -> 5, of which waited for: 4 -> 5; matrix products, arithmetic and copies ran while one was open for 10% -> 8% of each run, Pallas kernels for 0% -> 0%
where the time goes in v1:
time: 426 us; the launch traced here: 425 us
  waiting for transfers between devices  282 us (66%)
  matrix products  51 us (12%)
  local copies, waits for them, and re-layouts  40.5 us (10%)
  starting transfers between devices  36.1 us (8%)
  other arithmetic  14.3 us (3%)
    all_to_all x1, waiting for transfers between devices, per_device(): lax.all_to_all(jnp.stack([kv_weight] * lax.axis_size('dp')), 'dp', 0, 0)  181 us
    all_to_all x1, waiting for transfers between devices, per_device(): lax.all_to_all(keyval, 'sp', split_axis=1, concat_axis=0, tiled=True)  36.5 us
    all_to_all x1, waiting for transfers between devices, per_device(): lax.all_to_all(heads_out, 'sp', split_axis=0, concat_axis=1, tiled=True)  25.4 us
    all_to_all x1, waiting for transfers between devices, per_device(): lax.all_to_all(head_queries, 'sp', split_axis=1, concat_axis=0, tiled=True)  25.2 us
    dot_general x8, matrix products, attend(): jnp.einsum('hqk,khd->qhd', weights, values, preferred_element_type=jnp.fl...  18 us
    all_to_all x1, waiting for transfers between devices, copy_for_each(): lax.all_to_all(jnp.broadcast_to(value[None], (length, *value.shape)), axi...  14 us
    all_to_all x1, starting transfers between devices, copy_for_each(): lax.all_to_all(jnp.broadcast_to(value[None], (length, *value.shape)), axi...  11.7 us
    dot_general x8, matrix products, attend(): jnp.einsum('qhr,kr->hqk', query_block[..., NOPE:], keys_rotated, preferre...  11.4 us
  transfers between devices with their start and end apart: 5, of which 5 were waited for; matrix products, arithmetic and copies ran while one was open for 8% of the time, Pallas kernels for 0%

profile of v1, /device:TPU:8, one launch (start us, length us, event | category | flops | bytes accessed | tf_op | source)
XLA Modules:
  0.0 424.5 jit_solution(2765370649618298084)
XLA Ops:
  1.8 11.7 %all-to-all-start.3 = ((bf16[32,128,64]{1,2,0:T(8,128)(2,1)}), bf16[32,128,64]{1,2,0:T(8,128)(2,1)S(1)}, u32[]{:S(2)}, u32[]{:S(2)}) async-start(bf16[32,128,64]{1,2,0:T(8,128)(2,1)} %broadcast_in_dim.7), calls=%async_computation.3 | async-start | bytes 1048576 | tf_op jit(solution)/shard_map/all_to_all | solution.py:22
  13.5 2.9 copy.30
  16.4 14.0 %all-to-all-done.3 = bf16[32,128,64]{1,2,0:T(8,128)(2,1)S(1)} async-done(((bf16[32,128,64]{1,2,0:T(8,128)(2,1)}), bf16[32,128,64]{1,2,0:T(8,128)(2,1)S(1)}, u32[]{:S(2)}, u32[]{:S(2)}) %all-to-all-start.3) | async-done | bytes 524320 | tf_op jit(solution)/shard_map/all_to_all | solution.py:22
  30.4 6.0 %stack.2 = bf16[8,1024,1024]{1,2,0:T(8,128)(2,1)} broadcast(bf16[1024,1024]{0,1:T(8,128)(2,1)S(1)} %copy.30), dimensions={1,2} | broadcast | bytes 18874368 | tf_op jit(solution)/shard_map/stack | solution.py:76
  36.3 5.7 %all-to-all-start.1 = ((bf16[8,1024,1024]{1,2,0:T(8,128)(2,1)}), bf16[8,1024,1024]{1,2,0:T(8,128)(2,1)}, u32[]{:S(2)}, u32[]{:S(2)}) async-start(bf16[8,1024,1024]{1,2,0:T(8,128)(2,1)} %stack.2), calls=%async_computation.1 | async-start | bytes 33554432 | tf_op jit(solution)/shard_map/all_to_all | solution.py:76
  42.1 1.9 copy.28
  44.3 1.3 pad_maximum_fusion
  45.6 181.0 %all-to-all-done.1 = bf16[8,1024,1024]{1,2,0:T(8,128)(2,1)} async-done(((bf16[8,1024,1024]{1,2,0:T(8,128)(2,1)}), bf16[8,1024,1024]{1,2,0:T(8,128)(2,1)}, u32[]{:S(2)}, u32[]{:S(2)}) %all-to-all-start.1) | async-done | bytes 16777248 | tf_op jit(solution)/shard_map/all_to_all | solution.py:76
  226.5 5.6 %all-to-all-start = ((bf16[128,32,192]{0,2,1:T(8,128)(2,1)}), bf16[128,32,192]{0,2,1:T(8,128)(2,1)}, u32[]{:S(2)}, u32[]{:S(2)}) async-start(bf16[128,32,192]{0,2,1:T(8,128)(2,1)} %pad_maximum_fusion), calls=%async_computation | async-start | bytes 3145728 | tf_op jit(solution)/shard_map/all_to_all | solution.py:87
  232.3 11.3 %convolution_convert_fusion = bf16[128,8192]{1,0:T(8,128)(2,1)S(1)} fusion(bf16[1024,8192]{0,1:T(8,128)(2,1)} %bitcast.17, bf16[128,1024]{1,0:T(8,128)(2,1)S(1)} %copy-done.2, f32[1024]{0:T(1024)S(1)} %copy-done.7, f32[128]{0:T(128)S(1)} %add_rsqrt_fusion.1), kind=kOutput, calls=%fused_computation.16 | convolution fusion | flops 2149056512 | bytes 19141120 | tf_op jit(solution)/shard_map/dot_general | solution.py:73
  243.7 1.6 copy.42
  245.2 25.2 %all-to-all-done = bf16[128,32,192]{0,2,1:T(8,128)(2,1)} async-done(((bf16[128,32,192]{0,2,1:T(8,128)(2,1)}), bf16[128,32,192]{0,2,1:T(8,128)(2,1)}, u32[]{:S(2)}, u32[]{:S(2)}) %all-to-all-start) | async-done | bytes 1572896 | tf_op jit(solution)/shard_map/all_to_all | solution.py:87
  270.5 6.5 %all-to-all-start.2 = ((bf16[128,32,256]{2,0,1:T(8,128)(2,1)}), bf16[128,32,256]{2,0,1:T(8,128)(2,1)S(1)}, u32[]{:S(2)}, u32[]{:S(2)}) async-start(bf16[128,32,256]{2,0,1:T(8,128)(2,1)} %bitcast.90), calls=%async_computation.2 | async-start | bytes 4194304 | tf_op jit(solution)/shard_map/all_to_all | solution.py:88
  277.0 1.5 copy.38
  278.6 3.6 copy.29
  282.1 3.7 reshape.165
  285.9 3.1 copy.33
  288.9 36.5 %all-to-all-done.2 = bf16[128,32,256]{2,0,1:T(8,128)(2,1)S(1)} async-done(((bf16[128,32,256]{2,0,1:T(8,128)(2,1)}), bf16[128,32,256]{2,0,1:T(8,128)(2,1)S(1)}, u32[]{:S(2)}, u32[]{:S(2)}) %all-to-all-start.2) | async-done | bytes 2097184 | tf_op jit(solution)/shard_map/all_to_all | solution.py:88
  325.5 1.3 copy-done
  326.8 2.7 fusion.35
  329.5 57.8 %while.17 = (s32[]{:T(128)}, bf16[8,512,1,128]{3,1,2,0:T(8,128)(2,1)S(1)}, bf16[8,512,1,192]{1,3,2,0:T(8,128)(2,1)}, bf16[4096,1,128]{2,0,1:T(8,128)(2,1)S(1)}, ...) while((s32[]{:T(128)}, bf16[8,512,1,128]{3,1,2,0:T(8,128)(2,1)S(1)}, ...), condition=%wide.region_4.5_spmd, body=%wide.region_1.4_spmd.sunk | while | flops 1359019008 | bytes 50014320 | solution.py:101
  330.5 1.3 fusion.50
  331.8 1.4 fusion.51
  333.2 1.3 fusion.52
  334.5 2.2 fusion.53
  336.8 0.9 dynamic-slice_bitcast_fusion.2
  337.7 1.3 fusion.50
  339.0 1.4 fusion.51
  340.4 1.3 fusion.52
  341.7 2.2 fusion.53
  344.0 0.9 dynamic-slice_bitcast_fusion.2
  344.9 1.3 fusion.50
  346.2 1.4 fusion.51
  347.7 1.3 fusion.52
  349.0 2.2 fusion.53
  351.2 0.9 dynamic-slice_bitcast_fusion.2
  352.2 1.3 fusion.50
  353.5 1.4 fusion.51
  354.9 1.3 fusion.52
  356.2 2.2 fusion.53
  358.4 0.9 dynamic-slice_bitcast_fusion.2
  359.4 1.3 fusion.50
  360.7 1.4 fusion.51
  362.1 1.3 fusion.52
  363.4 2.2 fusion.53
  365.7 0.9 dynamic-slice_bitcast_fusion.2
  366.6 1.3 fusion.50
  367.9 1.4 fusion.51
  369.3 1.3 fusion.52
  370.6 2.2 fusion.53
  372.9 0.9 dynamic-slice_bitcast_fusion.2
  373.8 1.3 fusion.50
  375.1 1.4 fusion.51
  376.6 1.3 fusion.52
  377.9 2.2 fusion.53
  380.1 0.9 dynamic-slice_bitcast_fusion.2
  381.1 1.3 fusion.50
  382.4 1.4 fusion.51
  383.8 1.3 fusion.52
  385.1 2.2 fusion.53
  387.4 0.9 copy-done.5
  388.3 6.5 %all-to-all-start.4 = ((bf16[32,128,128]{2,1,0:T(8,128)(2,1)}), bf16[32,128,128]{2,1,0:T(8,128)(2,1)S(1)}, u32[]{:S(2)}, u32[]{:S(2)}) async-start(bf16[32,128,128]{2,1,0:T(8,128)(2,1)} %bitcast.93), calls=%async_computation.4 | async-start | bytes 2097152 | tf_op jit(solution)/shard_map/all_to_all | solution.py:115
  395.5 25.4 %all-to-all-done.4 = bf16[32,128,128]{2,1,0:T(8,128)(2,1)S(1)} async-done(((bf16[32,128,128]{2,1,0:T(8,128)(2,1)}), bf16[32,128,128]{2,1,0:T(8,128)(2,1)S(1)}, u32[]{:S(2)}, u32[]{:S(2)}) %all-to-all-start.4) | async-done | bytes 1048608 | tf_op jit(solution)/shard_map/all_to_all | solution.py:115
  423.2 1.3 copy.37
  (46 shorter events, 6.1 us)
Async XLA Ops:
  1.8 28.5 %all-to-all-start.3 = ((bf16[32,128,64]{1,2,0:T(8,128)(2,1)}), bf16[32,128,64]{1,2,0:T(8,128)(2,1)S(1)}, u32[]{:S(2)}, u32[]{:S(2)}) async-start(bf16[32,128,64]{1,2,0:T(8,128)(2,1)} %broadcast_in_dim.7), calls=%async_computation.3 | async-start | bytes 1048576 | tf_op jit(solution)/shard_map/all_to_all | solution.py:22
  30.4 6.0 %copy-start.1 = (bf16[32,128,64]{1,2,0:T(8,128)(2,1)}, bf16[32,128,64]{1,2,0:T(8,128)(2,1)S(1)}, u32[]{:S(2)}) copy-start(bf16[32,128,64]{1,2,0:T(8,128)(2,1)S(1)} %all-to-all-done.3) | copy-start | bytes 1572868
  36.3 190.2 %all-to-all-start.1 = ((bf16[8,1024,1024]{1,2,0:T(8,128)(2,1)}), bf16[8,1024,1024]{1,2,0:T(8,128)(2,1)}, u32[]{:S(2)}, u32[]{:S(2)}) async-start(bf16[8,1024,1024]{1,2,0:T(8,128)(2,1)} %stack.2), calls=%async_computation.1 | async-start | bytes 33554432 | tf_op jit(solution)/shard_map/all_to_all | solution.py:76
  45.6 186.6 %copy-start.2 = (bf16[128,1024]{1,0:T(8,128)(2,1)S(1)}, bf16[128,1024]{1,0:T(8,128)(2,1)}, u32[]{:S(2)}) copy-start(bf16[128,1024]{1,0:T(8,128)(2,1)} %param.10) | copy-start | bytes 786436
  45.6 186.8 %copy-start.7 = (f32[1024]{0:T(1024)S(1)}, f32[1024]{0:T(1024)}, u32[]{:S(2)}) copy-start(f32[1024]{0:T(1024)} %param.12) | copy-start | bytes 12292
  226.5 44.0 %all-to-all-start = ((bf16[128,32,192]{0,2,1:T(8,128)(2,1)}), bf16[128,32,192]{0,2,1:T(8,128)(2,1)}, u32[]{:S(2)}, u32[]{:S(2)}) async-start(bf16[128,32,192]{0,2,1:T(8,128)(2,1)} %pad_maximum_fusion), calls=%async_computation | async-start | bytes 3145728 | tf_op jit(solution)/shard_map/all_to_all | solution.py:87
  270.5 55.0 %all-to-all-start.2 = ((bf16[128,32,256]{2,0,1:T(8,128)(2,1)}), bf16[128,32,256]{2,0,1:T(8,128)(2,1)S(1)}, u32[]{:S(2)}, u32[]{:S(2)}) async-start(bf16[128,32,256]{2,0,1:T(8,128)(2,1)} %bitcast.90), calls=%async_computation.2 | async-start | bytes 4194304 | tf_op jit(solution)/shard_map/all_to_all | solution.py:88
  325.5 1.3 copy-start
  326.8 2.7 copy-start.4
  333.2 1.3 copy-start.6
  340.4 1.3 copy-start.6
  347.7 1.3 copy-start.6
  354.9 1.3 copy-start.6
  362.1 1.3 copy-start.6
  369.3 1.3 copy-start.6
  376.6 1.3 copy-start.6
  383.8 1.3 copy-start.6
  387.3 1.0 copy-start.5
  387.4 7.5 %copy-start.3 = (bf16[128,4096]{1,0:T(8,128)(2,1)S(1)}, bf16[128,4096]{1,0:T(8,128)(2,1)}, u32[]{:S(2)}) copy-start(bf16[128,4096]{1,0:T(8,128)(2,1)} %param.14) | copy-start | bytes 3145732
  388.3 32.6 %all-to-all-start.4 = ((bf16[32,128,128]{2,1,0:T(8,128)(2,1)}), bf16[32,128,128]{2,1,0:T(8,128)(2,1)S(1)}, u32[]{:S(2)}, u32[]{:S(2)}) async-start(bf16[32,128,128]{2,1,0:T(8,128)(2,1)} %bitcast.93), calls=%async_computation.4 | async-start | bytes 2097152 | tf_op jit(solution)/shard_map/all_to_all | solution.py:115
  395.5 26.9 %copy-start.8 = (f32[4096]{0:T(1024)S(1)}, f32[4096]{0:T(1024)}, u32[]{:S(2)}) copy-start(f32[4096]{0:T(1024)} %param.15) | copy-start | bytes 49156
